TPU v7x, 256 devices: a whole 4x4x8 slice. The times are simulated.
256 devices in a mesh: ep: 64 (over z, x, core), tp: 4 (over y).
Axes of the slice: x: 4, y: 4, z: 8, core: 2. Of those that a mesh axis runs over, the one named last changes fastest.
Arguments:
- queries: bfloat16 [16384, 8, 128], P('ep', 'tp'), may hold values from -256 to 256
- keys: bfloat16 [16384, 4, 128], P('ep', 'tp'), may hold values from -8 to 8
- values: bfloat16 [16384, 4, 128], P('ep', 'tp'), may hold values from -6 to 6
- attn_lambda: float32 [8], P('tp'), may hold values from 0.3 to 0.8
- head_gain: float32 [128], replicated, may hold values from 0.1 to 1.9
- w_out: bfloat16 [1024, 2048], replicated, may hold values from -0.1875 to 0.1875
- moe_rows: bfloat16 [32768, 2048], P('ep'), may hold values from -6 to 6
- moe_gain: float32 [2048], replicated, may hold values from 0.1 to 1.9
- routes: int32 [32768, 2], P('ep'), may hold values from 0 to 63, all different within a row; in each aligned block of 128 rows (0 to 127, 128 to 255, ...) at most 8 rows name the same one
- route_weights: float32 [32768, 2], P('ep'), may hold values from 0.1 to 1
- w_gate: bfloat16 [64, 2048, 1024], P('ep', None, 'tp'), may hold values from -0.125 to 0.125
- w_up: bfloat16 [64, 2048, 1024], P('ep', None, 'tp'), may hold values from -0.125 to 0.125
- w_down: bfloat16 [64, 1024, 2048], P('ep', 'tp'), may hold values from -0.1875 to 0.1875
Outputs:
- mixer_out: bfloat16 [16384, 2048], P(('ep', 'tp'))
- moe_out: bfloat16 [32768, 2048], P(('ep', 'tp'))
Inputs may be any that keep to these rules, and one draw needn't show every extreme that they name: `routes`: each row names 2 different experts. In each aligned block of 128 rows (the rows of moe_out that one device holds) no expert is named by more than 8 rows, a bound that some block reaches.
All inputs are finite; a program needn't handle non-finite values.
Results may differ from a plain program's by a relative error of at most 0.011.
Values may be sent and summed in bfloat16 or wider, within the bound.
No kernel may reach another device: no remote copies, remote signals or barrier semaphores. Data moves between devices by JAX's collectives and lax.ppermute only.
A program may use at most 128 MiB of HBM per device.

v0:
```python
import jax
import jax.numpy as jnp
from jax import lax
from jax.sharding import PartitionSpec as P

EPSILON = 1e-06
MASKED = -1e30


def split_up(x, dim, size):
    before, after = (x.shape[:dim], x.shape[dim + 1 :])
    return jnp.moveaxis(x.reshape(*before, size, -1, *after), dim, 0)


def sum_at_owner(x, axis, dim):
    size = lax.axis_size(axis)
    tiles = lax.all_to_all(split_up(x, dim, size), axis, 0, 0, tiled=True)
    return jnp.sum(tiles.astype(jnp.float32), axis=0)


def joined_along(tiles, dim):
    tiles = jnp.moveaxis(tiles, 0, dim)
    lengths = tiles.shape
    return tiles.reshape(*lengths[:dim], lengths[dim] * lengths[dim + 1], *lengths[dim + 2 :])


def piecewise(x, axis, dim, work, out_dim):
    span = x.shape[dim]
    pieces = jnp.split(x, 2, axis=dim) if span % 2 == 0 else [x]
    first = jnp.arange(lax.axis_size(axis)) * span
    tiles = [lax.all_gather(section, axis) for section in pieces]
    made = [jax.vmap(work)(b, first + k * (span // len(pieces))) for k, b in enumerate(tiles)]
    return joined_along(jnp.concatenate(made, axis=out_dim + 1), out_dim)


def rms_scaled(values_f, gain):
    mean_sq = jnp.mean(values_f * values_f, axis=-1, keepdims=True)
    return values_f * lax.rsqrt(mean_sq + EPSILON) * gain


def slot_numbers(block_routes, experts):
    flat_ids = block_routes.reshape(-1)
    matches = (flat_ids[:, None] == lax.iota(jnp.int32, experts)[None, :]).astype(jnp.int32)
    earlier = jnp.cumsum(matches, axis=0) - matches
    return jnp.sum(earlier * matches, axis=1).reshape(block_routes.shape)


def fill_slots(block_rows, block_routes, experts, capacity):
    slot_ids = slot_numbers(block_routes, experts)
    model_width = block_rows.shape[1]
    copies = jnp.broadcast_to(block_rows[:, None, :], block_routes.shape + (model_width,))
    blank_slots = jnp.zeros((experts, capacity, model_width), block_rows.dtype)
    return (blank_slots.at[block_routes, slot_ids].set(copies), slot_ids)


def local(
    queries,
    keys,
    values,
    attn_lambda,
    head_gain,
    w_out,
    moe_rows,
    moe_gain,
    routes,
    route_weights,
    w_gate,
    w_up,
    w_down,
):
    positions = queries.shape[0]
    q_heads = queries.shape[1]
    kv_heads = keys.shape[1]
    head_dim = queries.shape[2] // 2
    value_dim = values.shape[2]
    per_key = q_heads // kv_heads
    first_pos = lax.axis_index("ep") * positions
    query_pos = first_pos + lax.iota(jnp.int32, positions)
    last_pos = first_pos + positions - 1
    query_view = queries.reshape(positions, kv_heads, per_key, 2, head_dim)
    inv_scale = head_dim ** (-0.5)
    start_max = jnp.full((positions, kv_heads, per_key, 2), MASKED, jnp.float32)
    start_total = jnp.zeros((positions, kv_heads, per_key, 2), jnp.float32)
    start_acc = jnp.zeros((positions, kv_heads, per_key, 2, value_dim), jnp.float32)
    carry = (start_max, start_total, start_acc)
    key_piece = lax.all_gather(keys, "ep", axis=0, tiled=True)
    value_piece = lax.all_gather(values, "ep", axis=0, tiled=True)
    shard_count = key_piece.shape[0] // positions
    together = 1
    for candidate in (2, 3, 4):
        if shard_count % candidate == 0:
            together = candidate
    block_len = together * positions
    blocks = shard_count // together
    key_blocks = key_piece.reshape(blocks, block_len, kv_heads, 2, head_dim)
    value_blocks = value_piece.reshape(blocks, block_len, kv_heads, value_dim)
    block_starts = block_len * lax.iota(jnp.int32, blocks)

    def visit(running, inputs):
        key_blk, value_blk, block_start = inputs

        def update(current):
            run_max, run_total, run_acc = current
            key_pos = block_start + lax.iota(jnp.int32, block_len)
            scores = (
                jnp.einsum(
                    "qkgmd,pkmd->qkgmp", query_view, key_blk, preferred_element_type=jnp.float32
                )
                * inv_scale
            )
            allowed = key_pos[None, :] <= query_pos[:, None]
            scores = jnp.where(allowed[:, None, None, None, :], scores, MASKED)
            new_max = jnp.maximum(run_max, jnp.max(scores, axis=-1))
            shrink = jnp.exp(run_max - new_max)
            weights = jnp.exp(scores - new_max[..., None])
            run_total = run_total * shrink + jnp.sum(weights, axis=-1)
            run_acc = run_acc * shrink[..., None] + jnp.einsum(
                "qkgmp,pkv->qkgmv",
                weights.astype(jnp.bfloat16),
                value_blk,
                preferred_element_type=jnp.float32,
            )
            return (new_max, run_total, run_acc)

        def keep(current):
            return current

        return (lax.cond(block_start <= last_pos, update, keep, running), None)

    carry, unused = lax.scan(visit, carry, (key_blocks, value_blocks, block_starts))
    run_max, run_total, run_acc = carry
    ratios = run_acc / run_total[..., None]
    lambda_view = attn_lambda.reshape(1, kv_heads, per_key, 1)
    head_out = ratios[:, :, :, 0] - lambda_view * ratios[:, :, :, 1]
    attn_rows = (
        rms_scaled(head_out, head_gain).astype(jnp.bfloat16).reshape(positions, q_heads * value_dim)
    )
    tp_count = lax.axis_size("tp")
    tp_id = lax.axis_index("tp")
    head_width = q_heads * value_dim
    w_local = lax.dynamic_slice_in_dim(w_out, tp_id * head_width, head_width, 0)
    mixer_out = sum_at_owner(
        jnp.dot(attn_rows, w_local, preferred_element_type=jnp.float32).astype(jnp.bfloat16),
        "tp",
        0,
    ).astype(jnp.bfloat16)
    experts = lax.axis_size("ep")
    dev_rows = moe_rows.shape[0] // tp_count
    top_count = routes.shape[1]
    capacity = max(2, 2 * dev_rows * top_count // experts)
    model_width = moe_rows.shape[1]
    hidden_units = w_gate.shape[2]
    own_routes = lax.dynamic_slice_in_dim(routes, tp_id * dev_rows, dev_rows, 0)
    own_weights = lax.dynamic_slice_in_dim(route_weights, tp_id * dev_rows, dev_rows, 0)

    def expert_hidden(slot_rows):
        flat_rows = slot_rows.reshape(-1, model_width)
        gate_out = jnp.dot(flat_rows, w_gate[0], preferred_element_type=jnp.float32)
        up_out = jnp.dot(flat_rows, w_up[0], preferred_element_type=jnp.float32)
        return (
            (jax.nn.silu(gate_out) * up_out)
            .astype(jnp.bfloat16)
            .reshape(slot_rows.shape[:-1] + (hidden_units,))
        )

    own_rows = rms_scaled(
        lax.dynamic_slice_in_dim(moe_rows, tp_id * dev_rows, dev_rows, 0).astype(jnp.float32),
        moe_gain,
    ).astype(jnp.bfloat16)
    outgoing, own_slots = fill_slots(own_rows, own_routes, experts, capacity)
    arrived = lax.all_to_all(outgoing, "ep", split_axis=0, concat_axis=0, tiled=True)

    def hidden_piece(slot_rows, begin_row):
        return expert_hidden(slot_rows)

    hidden = piecewise(arrived[None], "tp", 0, hidden_piece, 0)
    all_units = lax.all_to_all(hidden, "tp", split_axis=0, concat_axis=3, tiled=True)
    down_whole = lax.all_gather(w_down[0], "tp", axis=0, tiled=True)
    flat_units = all_units.reshape(-1, tp_count * hidden_units)
    summed_f = jnp.zeros((flat_units.shape[0], model_width), jnp.float32)
    for group in range(tp_count):
        unit_block = flat_units[:, group * hidden_units : (group + 1) * hidden_units]
        weight_block = down_whole[group * hidden_units : (group + 1) * hidden_units]
        group_part = jnp.dot(unit_block, weight_block, preferred_element_type=jnp.float32).astype(
            jnp.bfloat16
        )
        summed_f = summed_f + group_part.astype(jnp.float32)
    summed = summed_f.astype(jnp.bfloat16).reshape(all_units.shape[:-1] + (model_width,))
    returned = lax.all_to_all(summed, "ep", split_axis=1, concat_axis=1, tiled=True)[0]
    picked = returned[own_routes, own_slots]
    moe_out = jnp.sum(own_weights[..., None] * picked.astype(jnp.float32), axis=1).astype(
        jnp.bfloat16
    )
    return (mixer_out, moe_out)


def solution(mesh):
    return jax.shard_map(
        local,
        mesh=mesh,
        in_specs=(
            P("ep", "tp", None),
            P("ep", "tp", None),
            P("ep", "tp", None),
            P("tp"),
            P(),
            P(),
            P("ep", None),
            P(),
            P("ep", None),
            P("ep", None),
            P("ep", None, "tp"),
            P("ep", None, "tp"),
            P("ep", "tp", None),
        ),
        out_specs=(P(("ep", "tp"), None), P(("ep", "tp"), None)),
        check_vma=False,
    )
```

profile of v0, /device:TPU:2, one launch (start us, length us, event | category | flops | bytes accessed | tf_op | source)
XLA Modules:
  0.0 434.8 jit_solution(10305571413842020620)
XLA Ops:
  7.2 0.7 all-gather.7.cloned.1.call-update
  8.0 0.7 all-gather.9.cloned.1.call-update
  8.7 0.7 constant_dynamic-slice_fusion
  9.8 0.6 reduce-window.6
  11.1 1.2 fusion.25
  12.3 1.3 fusion.27
  13.6 0.6 broadcast_in_dim.57
  14.2 1.2 reshape.247
  15.7 33.0 %scatter_fusion = bf16[64,8,2048]{2,1,0:T(8,128)(2,1)S(1)} fusion(bf16[64,8,2048]{2,1,0:T(8,128)(2,1)S(1)} %broadcast_in_dim.36, s32[256]{0:T(256)S(1)} %reshape.245, bf16[256,2048]{1,0:T(8,128)(2,1)} %reshape.247), kind=kCustom, calls=%fused_computation.1 | custom fusion | bytes 3147776 | tf_op jit(solution)/shard_map/scatter | solution.py:53
  48.8 73.1 %all_to_all.30 = bf16[64,8,2048]{2,1,0:T(8,128)(2,1)} all-to-all(bf16[64,8,2048]{2,1,0:T(8,128)(2,1)S(1)} %scatter_fusion), channel_id=1, replica_groups=mesh['ep'=64,'tp'=4] {'ep'}, dimensions={0} | all-to-all | bytes 4194304 | tf_op jit(solution)/shard_map/all_to_all | solution.py:171
  122.7 14.7 %reshape.263 = bf16[16,1024,1,2,64]{4,3,1,0,2:T(2,128)(2,1)} reshape(bf16[16384,1,128]{2,0,1:T(8,128)(2,1)} %all-gather.7.cloned.1.call-done) | data formatting | bytes 8388608 | tf_op jit(solution)/shard_map/reshape | solution.py:95
  137.4 20.2 %copy.37 = bf16[16,1024,1,2,64]{1,4,3,2,0:T(8,128)(2,1)} copy(bf16[16,1024,1,2,64]{4,3,1,0,2:T(2,128)(2,1)} %reshape.263) | data formatting | bytes 8388608
  157.6 29.6 %all-gather.9.cloned.1.call-done = bf16[16384,1,128]{2,0,1:T(8,128)(2,1)} async-done(((bf16[256,1,128]{2,0,1:T(8,128)(2,1)}), bf16[16384,1,128]{2,0,1:T(8,128)(2,1)}) %all-gather.9.cloned.1.call-update) | async-done | bytes 4194320 | tf_op jit(solution)/shard_map/all_gather | solution.py:87
  187.2 6.4 %copy.39 = bf16[16,1024,1,128]{1,3,2,0:T(8,128)(2,1)} copy(bf16[16,1024,1,128]{3,1,0,2:T(8,128)(2,1)} %bitcast.160) | data formatting | bytes 8388608
  193.6 23.8 %while.15 = (s32[]{:T(128)}, f32[256,1,2,2]{0,2,3,1:T(2,128)S(1)}, f32[256,1,2,2]{0,2,3,1:T(2,128)S(1)}, f32[256,1,2,2,128]{0,4,3,2,1:T(8,128)S(1)}, s32[16]{0:T...) while((s32[]{:T(128)}, f32[256,1,2,2]{0,2,3,1:T(2,128)S(1)}, ...), condition=%wide.region_5.6_spmd.clone, body=%wide.region_0.5_spmd.clone.sunk | while | flops 411570432 | bytes 15156511 | solution.py:130
  193.7 0.6 dynamic_slice.56
  194.8 5.2 %conditional.3 = ((f32[256,1,2,2]{0,2,3,1:T(2,128)S(1)}, f32[256,1,2,2]{0,2,3,1:T(2,128)S(1)}, f32[256,1,2,2,128]{0,4,3,2,1:T(8,128)S(1)})) conditional(s32[]{:T(128)} %convert_element_type.131, (f32[256,1,2,2]{0,2,3,1:T(2,128)S(1)}, f32[256,1,2,2]{0,2,3,1:T(2,128)S(1)}, f32[256,1,2,2,128]{0,4,3,2,1:T(8,128)S(1)}) %tuple.48, (s32[]{:T(128)}, ...), branch_computations={%region_1.1_spmd, %region_2.4_spmd} | conditional | flops 411570432 | bytes 15155240 | solution.py:128
  195.6 1.8 fusion.4
  197.4 1.0 fusion.5
  198.5 1.5 fusion.11
  200.0 0.6 dynamic_slice.56
  201.2 0.6 dynamic_slice.56
  202.3 0.6 dynamic_slice.56
  203.5 0.6 dynamic_slice.56
  204.7 0.6 dynamic_slice.56
  207.0 0.6 dynamic_slice.56
  208.2 0.6 dynamic_slice.56
  217.5 55.6 %all-gather.11.cloned.1.call-done = bf16[256,8,2048]{2,1,0:T(8,128)(2,1)} async-done(((bf16[64,8,2048]{2,1,0:T(8,128)(2,1)}), bf16[256,8,2048]{2,1,0:T(8,128)(2,1)}) %all-gather.11.cloned.1.call-update) | async-done | bytes 8388624 | tf_op jit(solution)/shard_map/all_gather | solution.py:31
  273.1 5.9 %fusion.28 = f32[4,512,256]{2,1,0:T(8,128)S(1)} fusion(bf16[4,512,2048]{2,1,0:T(8,128)(2,1)} %bitcast.170, bf16[1,2048,256]{2,1,0:T(8,128)(2,1)S(1)} %copy-done), kind=kOutput, calls=%fused_computation.47 | convolution fusion | flops 2147483648 | bytes 11534336 | tf_op jit(solution)/shard_map/vmap()/dot_general | solution.py:159
  279.1 3.6 fusion.24
  282.7 4.0 all-to-all-start.2
  287.0 2.8 convolution_convert_fusion.4
  289.8 22.2 %all-to-all-done.2 = bf16[4,64,8,256]{3,2,1,0:T(8,128)(2,1)S(1)} async-done(((bf16[4,64,8,256]{3,2,1,0:T(8,128)(2,1)}), bf16[4,64,8,256]{3,2,1,0:T(8,128)(2,1)S(1)}, u32[]{:S(2)}, u32[]{:S(2)}) %all-to-all-start.2) | async-done | bytes 1048608 | tf_op jit(solution)/shard_map/all_to_all | solution.py:177
  312.0 3.7 all-to-all-start
  315.7 1.4 copy.65
  317.3 29.3 %all-gather.13.cloned.1.call-done = bf16[1,1024,2048]{2,1,0:T(8,128)(2,1)} async-done(((bf16[1,256,2048]{2,1,0:T(8,128)(2,1)}), bf16[1,1024,2048]{2,1,0:T(8,128)(2,1)}) %all-gather.13.cloned.1.call-update) | async-done | bytes 4194320 | tf_op jit(solution)/shard_map/all_gather | solution.py:178
  346.6 2.1 convolution_convert_fusion
  348.7 1.9 convolution_convert_fusion.1
  350.7 0.7 convolution_convert_fusion.2
  351.4 2.6 fusion.23
  354.0 1.0 copy-done.2
  355.0 10.6 %all-to-all-start.3 = ((bf16[1,64,8,2048]{3,2,0,1:T(8,128)(2,1)}), bf16[1,64,8,2048]{3,2,0,1:T(8,128)(2,1)S(1)}, u32[]{:S(2)}, u32[]{:S(2)}) async-start(bf16[1,64,8,2048]{3,2,0,1:T(8,128)(2,1)} %fusion.23), calls=%async_computation.3 | async-start | bytes 4194304 | tf_op jit(solution)/shard_map/all_to_all | solution.py:189
  365.7 0.7 constant_dynamic-slice_fusion.1
  366.5 2.2 reduce_sum.60
  368.7 48.1 %all-to-all-done.3 = bf16[1,64,8,2048]{3,2,0,1:T(8,128)(2,1)S(1)} async-done(((bf16[1,64,8,2048]{3,2,0,1:T(8,128)(2,1)}), bf16[1,64,8,2048]{3,2,0,1:T(8,128)(2,1)S(1)}, u32[]{:S(2)}, u32[]{:S(2)}) %all-to-all-start.3) | async-done | bytes 2097184 | tf_op jit(solution)/shard_map/all_to_all | solution.py:189
  416.8 5.2 %gather_fusion = bf16[256,2048]{1,0:T(8,128)(2,1)} fusion(bf16[64,8,2048]{2,1,0:T(8,128)(2,1)S(1)} %bitcast.159, s32[256]{0:T(256)S(1)} %reshape.239), kind=kCustom, calls=%fused_computation | custom fusion | bytes 2099200 | tf_op jit(solution)/shard_map/gather | solution.py:190
  422.0 2.4 reshape.258
  424.4 3.9 multiply_reduce_fusion
  (98 shorter events, 8.7 us)
Async XLA Ops:
  7.2 266.0 %copy-start = (bf16[1,2048,256]{2,1,0:T(8,128)(2,1)S(1)}, bf16[1,2048,256]{2,1,0:T(8,128)(2,1)}, u32[]{:S(2)}) copy-start(bf16[1,2048,256]{2,1,0:T(8,128)(2,1)} %param.28) | copy-start | bytes 3145732
  7.2 115.6 %all-gather.7.cloned.1.call-start = ((), (), s32[]{:S(2)}) async-start(), calls=%async_computation.4 | async-start | bytes 4259840 | tf_op jit(solution)/shard_map/all_gather | solution.py:86
  7.9 179.3 %all-gather.9.cloned.1.call-start = ((), (), s32[]{:S(2)}) async-start(), calls=%async_computation.5 | async-start | bytes 4259840 | tf_op jit(solution)/shard_map/all_gather | solution.py:87
  8.7 264.5 %all-gather.11.cloned.1.call-start = ((), (), s32[]{:S(2)}) async-start(), calls=%async_computation.6 | async-start | bytes 10485760 | tf_op jit(solution)/shard_map/all_gather | solution.py:31
  48.7 73.8 %copy-start.3 = (bf16[256,2,128]{2,1,0:T(2,128)(2,1)S(1)}, bf16[256,2,128]{2,1,0:T(2,128)(2,1)}, u32[]{:S(2)}) copy-start(bf16[256,2,128]{2,1,0:T(2,128)(2,1)} %param.17) | copy-start | bytes 393220
  48.7 73.9 %copy-start.4 = (f32[2]{0:T(128)S(1)}, f32[2]{0:T(128)}, u32[]{:S(2)}) copy-start(f32[2]{0:T(128)} %param.20) | copy-start | bytes 28
  48.8 73.9 %copy-start.5 = (f32[128]{0:T(128)S(1)}, f32[128]{0:T(128)}, u32[]{:S(2)}) copy-start(f32[128]{0:T(128)} %param.21) | copy-start | bytes 1540
  121.9 224.7 %all-gather.13.cloned.1.call-start = ((), (), s32[]{:S(2)}) async-start(), calls=%async_computation.7 | async-start | bytes 5242880 | tf_op jit(solution)/shard_map/all_gather | solution.py:178
  273.1 5.9 %copy-start.6 = (bf16[256,8,2048]{2,1,0:T(8,128)(2,1)S(1)}, bf16[256,8,2048]{2,1,0:T(8,128)(2,1)}, u32[]{:S(2)}) copy-start(bf16[256,8,2048]{2,1,0:T(8,128)(2,1)} %all-gather.11.cloned.1.call-done) | copy-start | bytes 25165828
  273.1 6.0 %copy-start.7 = (bf16[1,2048,256]{2,1,0:T(8,128)(2,1)S(1)}, bf16[1,2048,256]{2,1,0:T(8,128)(2,1)}, u32[]{:S(2)}) copy-start(bf16[1,2048,256]{2,1,0:T(8,128)(2,1)} %param.27) | copy-start | bytes 3145732
  282.7 29.3 %all-to-all-start.2 = ((bf16[4,64,8,256]{3,2,1,0:T(8,128)(2,1)}), bf16[4,64,8,256]{3,2,1,0:T(8,128)(2,1)S(1)}, u32[]{:S(2)}, u32[]{:S(2)}) async-start(bf16[4,64,8,256]{3,2,1,0:T(8,128)(2,1)} %fusion.24), calls=%async_computation.2 | async-start | bytes 2097152 | tf_op jit(solution)/shard_map/all_to_all | solution.py:177
  312.0 42.0 %all-to-all-start = ((bf16[4,64,2048]{2,1,0:T(8,128)(2,1)}), bf16[4,64,2048]{2,1,0:T(8,128)(2,1)S(1)}, u32[]{:S(2)}, u32[]{:S(2)}) async-start(bf16[4,64,2048]{2,1,0:T(8,128)(2,1)} %bitcast.26), calls=%async_computation | async-start | bytes 2097152 | tf_op jit(solution)/shard_map/all_to_all | solution.py:17
  346.6 4.0 copy-start.1
  354.0 1.0 copy-start.2
  355.0 61.8 %all-to-all-start.3 = ((bf16[1,64,8,2048]{3,2,0,1:T(8,128)(2,1)}), bf16[1,64,8,2048]{3,2,0,1:T(8,128)(2,1)S(1)}, u32[]{:S(2)}, u32[]{:S(2)}) async-start(bf16[1,64,8,2048]{3,2,0,1:T(8,128)(2,1)} %fusion.23), calls=%async_computation.3 | async-start | bytes 4194304 | tf_op jit(solution)/shard_map/all_to_all | solution.py:189
Sparse Core Ops, SparseCore 0:
  10.8 94.4 all-gather.6
  108.0 79.1 all-gather.8
  189.0 84.0 all-gather.10
  274.8 71.7 all-gather.12
where the time goes:
time: 438 us; the launch traced here: 435 us
  waiting for transfers between devices  187 us (43%)
  local copies, waits for them, and re-layouts  98.3 us (22%)
  blocking collectives  73.1 us (17%)
  matrix products  23 us (5%)
  starting transfers between devices  18.6 us (4%)
  between operations  14.1 us (3%)
  other arithmetic  11.5 us (3%)
  loops' own time  9.72 us (2%)
    all_to_all x1, blocking collectives, local(): lax.all_to_all(outgoing, 'ep', split_axis=0, concat_axis=0, tiled=True)  73.1 us
    all_gather x1, waiting for transfers between devices, piecewise(): tiles = [lax.all_gather(section, axis) for section in pieces]  55.6 us
    all_to_all x1, waiting for transfers between devices, local(): lax.all_to_all(summed, 'ep', split_axis=1, concat_axis=1, tiled=True)[0]  48.1 us
    scatter x1, local copies, waits for them, and re-layouts, fill_slots(): return (blank_slots.at[block_routes, slot_ids].set(copies), slot_ids)  33 us
    all_gather x1, waiting for transfers between devices, local(): value_piece = lax.all_gather(values, 'ep', axis=0, tiled=True)  29.6 us
    all_gather x1, waiting for transfers between devices, local(): down_whole = lax.all_gather(w_down[0], 'tp', axis=0, tiled=True)  29.3 us
    unnamed x22, local copies, waits for them, and re-layouts  28.1 us
    all_to_all x1, waiting for transfers between devices, local(): lax.all_to_all(hidden, 'tp', split_axis=0, concat_axis=3, tiled=True)  22.2 us
  transfers between devices with their start and end apart: 7, of which 5 were waited for; matrix products, arithmetic and copies ran while one was open for 28% of the time, Pallas kernels for 0%

commit v1 on v0

--- a/solution.py
+++ b/solution.py
@@ -83,8 +83,15 @@
     start_total = jnp.zeros((positions, kv_heads, per_key, 2), jnp.float32)
     start_acc = jnp.zeros((positions, kv_heads, per_key, 2, value_dim), jnp.float32)
     carry = (start_max, start_total, start_acc)
-    key_piece = lax.all_gather(keys, "ep", axis=0, tiled=True)
-    value_piece = lax.all_gather(values, "ep", axis=0, tiled=True)
+
+    def edit_files(vec, body):
+        return jnp.split(
+            lax.all_gather(jnp.concatenate([body, vec], 1), "ep", tiled=True, axis=0),
+            [body.shape[1]],
+            1,
+        )
+
+    key_piece, value_piece = edit_files(values, keys)
     shard_count = key_piece.shape[0] // positions
     together = 1
     for candidate in (2, 3, 4):

time: 438 us -> 410 us (0.936)
  waiting for transfers between devices: 187 us -> 111 us
  starting transfers between devices: 18.6 us -> 45.9 us
  blocking collectives: 73.1 us -> 82.9 us
  local copies, waits for them, and re-layouts: 98.3 us -> 105 us
    all_gather x1, waiting for transfers between devices: 55.6 us -> 11.3 us  [piecewise(): tiles = [lax.all_gather(section, axis) for section in pieces]]
    all_gather x2 -> x1, waiting for transfers between devices: 29.6 us -> 0.01 us  [edit_files(): lax.all_gather(jnp.concatenate([body, vec], 1), 'ep', tiled=True, axis=0)]
    all_to_all x1, starting transfers between devices: 10.6 us -> 37.9 us  [local(): lax.all_to_all(summed, 'ep', split_axis=1, concat_axis=1, tiled=True)[0]]
    all_to_all x1, blocking collectives: 73.1 us -> 82.9 us  [local(): lax.all_to_all(outgoing, 'ep', split_axis=0, concat_axis=0, tiled=True)]
    split x0 -> x1, local copies, waits for them, and re-layouts: none -> 5.8 us  [edit_files(): jnp.split(lax.all_gather(jnp.concatenate([body, vec], 1), 'ep', tiled=Tru...]
  transfers between devices with their start and end apart: 7 -> 6, of which waited for: 5 -> 4; matrix products, arithmetic and copies ran while one was open for 28% -> 31% of each run, Pallas kernels for 0% -> 0%
where the time goes in v1:
time: 410 us; the launch traced here: 407 us
  waiting for transfers between devices  111 us (27%)
  local copies, waits for them, and re-layouts  105 us (26%)
  blocking collectives  82.9 us (20%)
  starting transfers between devices  45.9 us (11%)
  matrix products  22.9 us (6%)
  between operations  14.1 us (3%)
  other arithmetic  13.2 us (3%)
  loops' own time  11.1 us (3%)
    all_to_all x1, blocking collectives, local(): lax.all_to_all(outgoing, 'ep', split_axis=0, concat_axis=0, tiled=True)  82.9 us
    all_to_all x1, waiting for transfers between devices, local(): lax.all_to_all(summed, 'ep', split_axis=1, concat_axis=1, tiled=True)[0]  48.1 us
    all_to_all x1, starting transfers between devices, local(): lax.all_to_all(summed, 'ep', split_axis=1, concat_axis=1, tiled=True)[0]  37.9 us
    scatter x1, local copies, waits for them, and re-layouts, fill_slots(): return (blank_slots.at[block_routes, slot_ids].set(copies), slot_ids)  33 us
    all_gather x1, waiting for transfers between devices, local(): down_whole = lax.all_gather(w_down[0], 'tp', axis=0, tiled=True)  29.4 us
    unnamed x22, local copies, waits for them, and re-layouts  28.2 us
    all_to_all x1, waiting for transfers between devices, local(): lax.all_to_all(hidden, 'tp', split_axis=0, concat_axis=3, tiled=True)  22.1 us
    reshape x1, local copies, waits for them, and re-layouts, local(): key_blocks = key_piece.reshape(blocks, block_len, kv_heads, 2, head_dim)  14.8 us
  transfers between devices with their start and end apart: 6, of which 4 were waited for; matrix products, arithmetic and copies ran while one was open for 31% of the time, Pallas kernels for 0%

profile of v1, /device:TPU:2, one launch (start us, length us, event | category | flops | bytes accessed | tf_op | source)
XLA Modules:
  0.0 406.5 jit_solution(16740434606799057168)
XLA Ops:
  7.2 1.6 pad_maximum_fusion
  8.9 0.7 constant_dynamic-slice_fusion
  10.0 0.6 reduce-window.6
  11.3 1.2 fusion.25
  12.6 1.3 fusion.27
  13.8 0.6 broadcast_in_dim.57
  14.4 1.2 reshape.247
  15.9 33.0 %scatter_fusion = bf16[64,8,2048]{2,1,0:T(8,128)(2,1)S(1)} fusion(bf16[64,8,2048]{2,1,0:T(8,128)(2,1)S(1)} %broadcast_in_dim.36, s32[256]{0:T(256)S(1)} %reshape.245, bf16[256,2048]{1,0:T(8,128)(2,1)} %reshape.247), kind=kCustom, calls=%fused_computation.1 | custom fusion | bytes 3147776 | tf_op jit(solution)/shard_map/scatter | solution.py:53
  49.0 82.9 %all_to_all.30 = bf16[64,8,2048]{2,1,0:T(8,128)(2,1)} all-to-all(bf16[64,8,2048]{2,1,0:T(8,128)(2,1)S(1)} %scatter_fusion), channel_id=1, replica_groups=mesh['ep'=64,'tp'=4] {'ep'}, dimensions={0} | all-to-all | bytes 4194304 | tf_op jit(solution)/shard_map/all_to_all | solution.py:178
  132.9 5.8 %fusion.50 = (bf16[16384,1,128]{2,0,1:T(8,128)(2,1)}, bf16[16384,1,128]{2,0,1:T(8,128)(2,1)}) fusion(bf16[16384,2,128]{2,0,1:T(8,128)(2,1)} %all-gather.6.cloned.1.call-done), kind=kLoop, calls=%fused_computation.94 | loop fusion | bytes 16777216 | tf_op jit(solution)/shard_map/split | solution.py:88
  138.7 14.8 %reshape.263 = bf16[16,1024,1,2,64]{4,3,1,0,2:T(2,128)(2,1)} reshape(bf16[16384,1,128]{2,0,1:T(8,128)(2,1)} %get-tuple-element.216) | data formatting | bytes 8388608 | tf_op jit(solution)/shard_map/reshape | solution.py:102
  153.5 20.2 %copy.37 = bf16[16,1024,1,2,64]{1,4,3,2,0:T(8,128)(2,1)} copy(bf16[16,1024,1,2,64]{4,3,1,0,2:T(2,128)(2,1)} %reshape.263) | data formatting | bytes 8388608
  173.7 6.4 %copy.39 = bf16[16,1024,1,128]{1,3,2,0:T(8,128)(2,1)} copy(bf16[16,1024,1,128]{3,1,0,2:T(8,128)(2,1)} %bitcast.160) | data formatting | bytes 8388608
  180.2 25.8 %while.15 = (s32[]{:T(128)}, f32[256,1,2,2]{0,2,3,1:T(2,128)S(1)}, f32[256,1,2,2]{0,2,3,1:T(2,128)S(1)}, f32[256,1,2,2,128]{0,4,3,2,1:T(8,128)S(1)}, s32[16]{0:T...) while((s32[]{:T(128)}, f32[256,1,2,2]{0,2,3,1:T(2,128)S(1)}, ...), condition=%wide.region_5.6_spmd.clone, body=%wide.region_0.5_spmd.clone.sunk | while | flops 411570432 | bytes 15156503 | solution.py:137
  180.2 0.6 dynamic_slice.56
  181.5 5.3 %conditional.3 = ((f32[256,1,2,2]{0,2,3,1:T(2,128)S(1)}, f32[256,1,2,2]{0,2,3,1:T(2,128)S(1)}, f32[256,1,2,2,128]{0,4,3,2,1:T(8,128)S(1)})) conditional(s32[]{:T(128)} %convert_element_type.131, (f32[256,1,2,2]{0,2,3,1:T(2,128)S(1)}, f32[256,1,2,2]{0,2,3,1:T(2,128)S(1)}, f32[256,1,2,2,128]{0,4,3,2,1:T(8,128)S(1)}) %tuple.49, (s32[]{:T(128)}, ...), branch_computations={%region_1.1_spmd, %region_2.4_spmd} | conditional | flops 411570432 | bytes 15155240 | solution.py:135
  181.5 0.7 iota_add_fusion
  182.4 1.8 fusion.4
  184.2 1.0 fusion.5
  185.2 1.5 fusion.11
  186.8 0.6 dynamic_slice.56
  188.1 0.6 dynamic_slice.56
  189.3 0.6 dynamic_slice.56
  190.6 0.6 dynamic_slice.56
  191.9 0.6 dynamic_slice.56
  195.7 0.6 dynamic_slice.56
  197.0 0.6 dynamic_slice.56
  206.0 11.3 %all-gather.8.cloned.1.call-done = bf16[256,8,2048]{2,1,0:T(8,128)(2,1)} async-done(((bf16[64,8,2048]{2,1,0:T(8,128)(2,1)}), bf16[256,8,2048]{2,1,0:T(8,128)(2,1)}) %all-gather.8.cloned.1.call-update) | async-done | bytes 8388624 | tf_op jit(solution)/shard_map/all_gather | solution.py:31
  217.4 5.9 %fusion.28 = f32[4,512,256]{2,1,0:T(8,128)S(1)} fusion(bf16[4,512,2048]{2,1,0:T(8,128)(2,1)} %bitcast.170, bf16[1,2048,256]{2,1,0:T(8,128)(2,1)S(1)} %copy-done), kind=kOutput, calls=%fused_computation.47 | convolution fusion | flops 2147483648 | bytes 11534336 | tf_op jit(solution)/shard_map/vmap()/dot_general | solution.py:166
  223.4 3.6 fusion.24
  227.0 4.0 all-to-all-start.2
  231.3 2.8 convolution_convert_fusion.4
  234.1 22.1 %all-to-all-done.2 = bf16[4,64,8,256]{3,2,1,0:T(8,128)(2,1)S(1)} async-done(((bf16[4,64,8,256]{3,2,1,0:T(8,128)(2,1)}), bf16[4,64,8,256]{3,2,1,0:T(8,128)(2,1)S(1)}, u32[]{:S(2)}, u32[]{:S(2)}) %all-to-all-start.2) | async-done | bytes 1048608 | tf_op jit(solution)/shard_map/all_to_all | solution.py:184
  256.1 3.7 all-to-all-start
  259.9 1.4 copy.65
  261.4 29.4 %all-gather.10.cloned.1.call-done = bf16[1,1024,2048]{2,1,0:T(8,128)(2,1)} async-done(((bf16[1,256,2048]{2,1,0:T(8,128)(2,1)}), bf16[1,1024,2048]{2,1,0:T(8,128)(2,1)}) %all-gather.10.cloned.1.call-update) | async-done | bytes 4194320 | tf_op jit(solution)/shard_map/all_gather | solution.py:185
  290.9 2.1 convolution_convert_fusion
  293.0 1.9 convolution_convert_fusion.1
  294.9 0.7 convolution_convert_fusion.2
  295.7 2.6 fusion.23
  298.3 1.0 copy-done.2
  299.3 37.9 %all-to-all-start.3 = ((bf16[1,64,8,2048]{3,2,0,1:T(8,128)(2,1)}), bf16[1,64,8,2048]{3,2,0,1:T(8,128)(2,1)S(1)}, u32[]{:S(2)}, u32[]{:S(2)}) async-start(bf16[1,64,8,2048]{3,2,0,1:T(8,128)(2,1)} %fusion.23), calls=%async_computation.3 | async-start | bytes 4194304 | tf_op jit(solution)/shard_map/all_to_all | solution.py:196
  337.3 0.7 constant_dynamic-slice_fusion.1
  338.1 2.2 reduce_sum.60
  340.3 48.1 %all-to-all-done.3 = bf16[1,64,8,2048]{3,2,0,1:T(8,128)(2,1)S(1)} async-done(((bf16[1,64,8,2048]{3,2,0,1:T(8,128)(2,1)}), bf16[1,64,8,2048]{3,2,0,1:T(8,128)(2,1)S(1)}, u32[]{:S(2)}, u32[]{:S(2)}) %all-to-all-start.3) | async-done | bytes 2097184 | tf_op jit(solution)/shard_map/all_to_all | solution.py:196
  388.4 5.2 %gather_fusion = bf16[256,2048]{1,0:T(8,128)(2,1)} fusion(bf16[64,8,2048]{2,1,0:T(8,128)(2,1)S(1)} %bitcast.159, s32[256]{0:T(256)S(1)} %reshape.239), kind=kCustom, calls=%fused_computation | custom fusion | bytes 2099200 | tf_op jit(solution)/shard_map/gather | solution.py:197
  393.7 2.4 reshape.258
  396.0 3.9 multiply_reduce_fusion
  (97 shorter events, 8.5 us)
Async XLA Ops:
  7.2 210.2 %copy-start = (bf16[1,2048,256]{2,1,0:T(8,128)(2,1)S(1)}, bf16[1,2048,256]{2,1,0:T(8,128)(2,1)}, u32[]{:S(2)}) copy-start(bf16[1,2048,256]{2,1,0:T(8,128)(2,1)} %param.28) | copy-start | bytes 3145732
  7.2 125.8 %all-gather.6.cloned.1.call-start = ((), (), s32[]{:S(2)}) async-start(), calls=%async_computation.4 | async-start | bytes 8519680 | tf_op jit(solution)/shard_map/all_gather | solution.py:89
  8.9 208.5 %all-gather.8.cloned.1.call-start = ((), (), s32[]{:S(2)}) async-start(), calls=%async_computation.5 | async-start | bytes 10485760 | tf_op jit(solution)/shard_map/all_gather | solution.py:31
  48.9 83.8 %copy-start.3 = (bf16[256,2,128]{2,1,0:T(2,128)(2,1)S(1)}, bf16[256,2,128]{2,1,0:T(2,128)(2,1)}, u32[]{:S(2)}) copy-start(bf16[256,2,128]{2,1,0:T(2,128)(2,1)} %param.17) | copy-start | bytes 393220
  49.0 83.9 %copy-start.4 = (f32[2]{0:T(128)S(1)}, f32[2]{0:T(128)}, u32[]{:S(2)}) copy-start(f32[2]{0:T(128)} %param.20) | copy-start | bytes 28
  49.0 83.9 %copy-start.5 = (f32[128]{0:T(128)S(1)}, f32[128]{0:T(128)}, u32[]{:S(2)}) copy-start(f32[128]{0:T(128)} %param.21) | copy-start | bytes 1540
  131.9 158.9 %all-gather.10.cloned.1.call-start = ((), (), s32[]{:S(2)}) async-start(), calls=%async_computation.6 | async-start | bytes 5242880 | tf_op jit(solution)/shard_map/all_gather | solution.py:185
  217.4 5.9 %copy-start.6 = (bf16[256,8,2048]{2,1,0:T(8,128)(2,1)S(1)}, bf16[256,8,2048]{2,1,0:T(8,128)(2,1)}, u32[]{:S(2)}) copy-start(bf16[256,8,2048]{2,1,0:T(8,128)(2,1)} %all-gather.8.cloned.1.call-done) | copy-start | bytes 25165828
  217.4 6.0 %copy-start.7 = (bf16[1,2048,256]{2,1,0:T(8,128)(2,1)S(1)}, bf16[1,2048,256]{2,1,0:T(8,128)(2,1)}, u32[]{:S(2)}) copy-start(bf16[1,2048,256]{2,1,0:T(8,128)(2,1)} %param.27) | copy-start | bytes 3145732
  227.0 29.1 %all-to-all-start.2 = ((bf16[4,64,8,256]{3,2,1,0:T(8,128)(2,1)}), bf16[4,64,8,256]{3,2,1,0:T(8,128)(2,1)S(1)}, u32[]{:S(2)}, u32[]{:S(2)}) async-start(bf16[4,64,8,256]{3,2,1,0:T(8,128)(2,1)} %fusion.24), calls=%async_computation.2 | async-start | bytes 2097152 | tf_op jit(solution)/shard_map/all_to_all | solution.py:184
  256.1 42.1 %all-to-all-start = ((bf16[4,64,2048]{2,1,0:T(8,128)(2,1)}), bf16[4,64,2048]{2,1,0:T(8,128)(2,1)S(1)}, u32[]{:S(2)}, u32[]{:S(2)}) async-start(bf16[4,64,2048]{2,1,0:T(8,128)(2,1)} %bitcast.26), calls=%async_computation | async-start | bytes 2097152 | tf_op jit(solution)/shard_map/all_to_all | solution.py:17
  290.9 4.0 copy-start.1
  298.3 1.0 copy-start.2
  299.3 89.2 %all-to-all-start.3 = ((bf16[1,64,8,2048]{3,2,0,1:T(8,128)(2,1)}), bf16[1,64,8,2048]{3,2,0,1:T(8,128)(2,1)S(1)}, u32[]{:S(2)}, u32[]{:S(2)}) async-start(bf16[1,64,8,2048]{3,2,0,1:T(8,128)(2,1)} %fusion.23), calls=%async_computation.3 | async-start | bytes 4194304 | tf_op jit(solution)/shard_map/all_to_all | solution.py:196
Sparse Core Ops, SparseCore 0:
  11.4 118.0 all-gather.5
  132.1 85.2 all-gather.7
  219.2 71.6 all-gather.9
